TPU v7x, 512 devices: a whole 4x4x16 slice. The times are simulated.
512 devices in a mesh: sp: 32 (over z, core), tp: 16 (over y, x).
Axes of the slice: x: 4, y: 4, z: 16, core: 2. Of those that a mesh axis runs over, the one named last changes fastest.
Arguments:
- query_rows: bfloat16 [16384, 1024], P('sp', 'tp'), may hold values from -128 to 128
- key_rows: bfloat16 [16384, 1024], P('sp', 'tp'), may hold values from -4 to 4
- value_rows: bfloat16 [16384, 1024], P('sp', 'tp'), may hold values from -6 to 6
- cum_gates: float32 [16384, 16], P('sp', 'tp'), may hold values from -16386 to 0, as said below
- residual: bfloat16 [16384, 2048], P('sp', 'tp'), may hold values from -64 to 64
- output_weight: bfloat16 [1024, 2048], P(None, 'tp'), may hold values from -0.1875 to 0.1875
- norm_gain: bfloat16 [2048], replicated, may hold values from 0.099609375 to 1.8984375
- expert_index: int32 [16384, 2], P('sp'), may hold values from 0 to 31, all different within a row; in each aligned block of 512 rows (0 to 511, 512 to 1023, ...) at most 64 rows name the same one
- route_weights: float32 [16384, 2], P('sp'), may hold values from 0.2 to 1
- gate_weight: bfloat16 [32, 2048, 2048], P('sp', None, 'tp'), may hold values from -2 to 2
- up_weight: bfloat16 [32, 2048, 2048], P('sp', None, 'tp'), may hold values from -2 to 2
- down_weight: bfloat16 [32, 2048, 2048], P('sp', None, 'tp'), may hold values from -0.125 to 0.125
Outputs:
- layer_out: bfloat16 [16384, 2048], P('sp', 'tp')
Inputs may be any that keep to these rules, and one draw needn't show every extreme that they name: `cum_gates`: each head's values never rise along positions. `expert_index`: each token names 2 different experts. In the 512 tokens of one index of sp no expert is named more than 64 times, and in some index's tokens some expert is named exactly 64 times.
All inputs are finite; a program needn't handle non-finite values.
Results may differ from a plain program's by a relative error of at most 0.01.
Values may be sent and summed in bfloat16 or wider, within the bound.
A program may use at most 64 MiB of HBM per device.

v0:
```python
import math
import jax
import jax.numpy as jnp
from jax import lax
from jax.sharding import PartitionSpec as P

NORM_EPS = 1e-06
CLAMP_LIMIT = 7.0
SILU_ALPHA = 1.702


def joined_along(parts, dim):
    lengths = list(parts.shape[1:])
    lengths[dim] *= parts.shape[0]
    return jnp.moveaxis(parts, 0, dim).reshape(lengths)


def copy_for_each(x, axis):
    copies = jnp.broadcast_to(x, (lax.axis_size(axis), *x.shape))
    return lax.all_to_all(copies, axis, split_axis=0, concat_axis=0, tiled=True)


def gathered_copies(x, axis, dim):
    return joined_along(copy_for_each(x, axis), dim)


def side_by_side(arrays, axis, dim, along):
    widths = [a.shape[along] for a in arrays]
    both = jnp.concatenate(arrays, axis=along)
    result = lax.all_gather(both, axis, axis=dim, tiled=True)
    return tuple(jnp.split(result, [sum(widths[:k]) for k in range(1, len(widths))], axis=along))


def normalize(rows, norm_gain):
    wide = rows.astype(jnp.float32)
    factor = lax.rsqrt(jnp.mean(wide * wide, axis=-1, keepdims=True) + NORM_EPS)
    return (wide * factor * norm_gain.astype(jnp.float32)).astype(jnp.bfloat16)


def attend_local(query_rows, key_rows, value_rows, cum_gates):
    rows = query_rows.shape[0]
    heads_here = cum_gates.shape[1]
    head_size = query_rows.shape[1] // heads_here
    first_place = lax.axis_index("sp") * rows
    all_gates = gathered_copies(cum_gates, "sp", 0)
    queries = query_rows.reshape(rows, heads_here, head_size)
    query_place = first_place + jnp.arange(rows, dtype=jnp.int32)
    root_scale = head_size ** (-0.5)
    start_state = (
        jnp.full((rows, heads_here), -jnp.inf, jnp.float32),
        jnp.zeros((rows, heads_here), jnp.float32),
        jnp.zeros((rows, heads_here, head_size), jnp.float32),
    )
    key_piece, value_piece = side_by_side((key_rows, value_rows), "sp", 0, 1)
    count = key_piece.shape[0]
    block = math.gcd(count, 512)

    def one_block(number, state):
        top, total, summed = state
        offset = number * block
        key_block = lax.dynamic_slice_in_dim(key_piece, number * block, block, 0).reshape(
            block, heads_here, head_size
        )
        value_block = lax.dynamic_slice_in_dim(value_piece, number * block, block, 0).reshape(
            block, heads_here, head_size
        )
        gate_block = lax.dynamic_slice_in_dim(all_gates, offset, block, 0)
        scores = (
            jnp.einsum("qhd,khd->qhk", queries, key_block, preferred_element_type=jnp.float32)
            * root_scale
        )
        scores = scores + cum_gates[:, :, None] - gate_block.T[None, :, :]
        key_place = offset + jnp.arange(block, dtype=jnp.int32)
        allowed = key_place[None, :] <= query_place[:, None]
        scores = jnp.where(allowed[:, None, :], scores, -jnp.inf)
        new_top = jnp.maximum(top, jnp.max(scores, axis=-1))
        safe_top = jnp.where(new_top == -jnp.inf, 0.0, new_top)
        raised = jnp.exp(scores - safe_top[:, :, None])
        shrink = jnp.exp(top - safe_top)
        total = total * shrink + jnp.sum(raised, axis=-1)
        summed = summed * shrink[:, :, None] + jnp.einsum(
            "qhk,khd->qhd",
            raised.astype(jnp.bfloat16),
            value_block,
            preferred_element_type=jnp.float32,
        )
        return (new_top, total, summed)

    def compute(state):
        return lax.fori_loop(0, count // block, one_block, state)

    def keep_state(state):
        return state

    top, total, summed = lax.cond(
        jnp.int32(0) <= first_place + rows - 1, compute, keep_state, start_state
    )
    return (summed / total[:, :, None]).astype(jnp.bfloat16).reshape(rows, heads_here * head_size)


def body(
    query_rows,
    key_rows,
    value_rows,
    cum_gates,
    residual,
    output_weight,
    norm_gain,
    expert_index,
    route_weights,
    gate_weight,
    up_weight,
    down_weight,
):
    attended = attend_local(query_rows, key_rows, value_rows, cum_gates)
    weight_rows = output_weight
    projected = jnp.dot(
        gathered_copies(attended, "tp", 1), weight_rows, preferred_element_type=jnp.float32
    )
    mixed = (residual.astype(jnp.float32) + projected).astype(jnp.bfloat16)
    rows = residual.shape[0]
    topk = expert_index.shape[1]
    local_experts = gate_weight.shape[0]
    groups = lax.axis_size("sp")
    experts = local_experts * groups
    capacity = 2 * rows * topk // experts
    chosen = expert_index.reshape(rows * topk)
    matches = (chosen[:, None] == jnp.arange(experts, dtype=jnp.int32)[None, :]).astype(jnp.int32)
    rank = jnp.sum((jnp.cumsum(matches, axis=0) - matches) * matches, axis=1)
    slot = chosen * capacity + rank
    owner = jnp.arange(rows * topk, dtype=jnp.int32) // topk
    slot_token = jnp.full((experts * capacity,), rows, jnp.int32).at[slot].set(owner)
    padded = jnp.concatenate([mixed, jnp.zeros((1, mixed.shape[1]), mixed.dtype)], axis=0)
    outgoing = padded[slot_token].reshape(experts, capacity, mixed.shape[1])
    arrived = lax.all_to_all(outgoing, "sp", split_axis=0, concat_axis=0, tiled=True)
    count = arrived.shape[1]
    grouped = arrived.reshape(groups, local_experts, count, arrived.shape[2])
    normed = normalize(lax.all_gather(grouped, "tp", axis=3, tiled=True), norm_gain)
    gate_input = jnp.einsum(
        "seid,edf->seif", normed, gate_weight, preferred_element_type=jnp.float32
    )
    linear_input = jnp.einsum(
        "seid,edf->seif", normed, up_weight, preferred_element_type=jnp.float32
    )
    gate_cut = jnp.minimum(gate_input, CLAMP_LIMIT)
    linear_cut = jnp.clip(linear_input, -CLAMP_LIMIT, CLAMP_LIMIT)
    activated = (gate_cut * jax.nn.sigmoid(SILU_ALPHA * gate_cut) * (linear_cut + 1.0)).astype(
        jnp.bfloat16
    )
    weight_rows = down_weight
    produced = jnp.einsum(
        "seif,efc->seic",
        lax.all_gather(activated, "tp", axis=3, tiled=True),
        weight_rows,
        preferred_element_type=jnp.float32,
    ).astype(jnp.bfloat16)
    returned = lax.all_to_all(
        produced.reshape(groups * local_experts, count, down_weight.shape[2]),
        "sp",
        split_axis=0,
        concat_axis=0,
        tiled=True,
    )
    flat = returned.reshape(experts * capacity, returned.shape[2])
    picked = flat[slot].reshape(rows, topk, flat.shape[1]).astype(jnp.float32)
    blended = jnp.sum(route_weights[:, :, None] * picked, axis=1)
    return (mixed.astype(jnp.float32) + blended).astype(jnp.bfloat16)


def solution(mesh):
    placed = (
        P("sp", "tp"),
        P("sp", "tp"),
        P("sp", "tp"),
        P("sp", "tp"),
        P("sp", "tp"),
        P(None, "tp"),
        P(),
        P("sp", None),
        P("sp", None),
        P("sp", None, "tp"),
        P("sp", None, "tp"),
        P("sp", None, "tp"),
    )
    return jax.shard_map(body, mesh=mesh, in_specs=placed, out_specs=P("sp", "tp"), check_vma=False)
```

profile of v0, /device:TPU:1, one launch (start us, length us, event | category | flops | bytes accessed | tf_op | source)
XLA Modules:
  0.0 568.3 jit_solution(3906957129772426121)
XLA Ops:
  9.3 1.3 broadcast_in_dim.66
  10.7 16.7 %all-to-all-start = ((f32[32,512,1]{1,2,0:T(1,128)}), f32[32,512,1]{1,2,0:T(1,128)S(1)}, u32[]{:S(2)}, u32[]{:S(2)}) async-start(f32[32,512,1]{1,2,0:T(1,128)} %broadcast_in_dim.66), calls=%async_computation | async-start | bytes 131072 | tf_op jit(solution)/shard_map/all_to_all | solution.py:20
  28.4 12.0 %all-to-all-done = f32[32,512,1]{1,2,0:T(1,128)S(1)} async-done(((f32[32,512,1]{1,2,0:T(1,128)}), f32[32,512,1]{1,2,0:T(1,128)S(1)}, u32[]{:S(2)}, u32[]{:S(2)}) %all-to-all-start) | async-done | bytes 65568 | tf_op jit(solution)/shard_map/all_to_all | solution.py:20
  40.4 48.2 %all-gather.5.cloned.1.call-done = bf16[16384,128]{1,0:T(8,128)(2,1)} async-done(((bf16[512,128]{1,0:T(8,128)(2,1)}), bf16[16384,128]{1,0:T(8,128)(2,1)}) %all-gather.5.cloned.1.call-update) | async-done | bytes 4194320 | tf_op jit(solution)/shard_map/all_gather | solution.py:30
  88.6 153.3 %conditional.1 = (f32[512,1]{0,1:T(1,128)}, f32[512,1,64]{0,2,1:T(8,128)}) conditional(s32[]{:T(128)} %convert_element_type.57, () %tuple.27, (bf16[16384,128]{1,0:T(8,128)(2,1)}, f32[32,512,1]{1,2,0:T(1,128)S(1)}, bf16[512,64]{0,1:T(8,128)(2,1)}, s32[]{:T(128)}, s32[512]{0:T(512)S(1)}, /*index=5*/f32[512,1]{0,1:T(1,128)}) %tuple.28), branch_computations={%region_0.0_spmd, %region_1.6_spmd} | conditional | flops 69834240 | bytes 12448155 | solution.py:95
  88.7 7.3 %fusion.71 = (bf16[16384,64]{1,0:T(8,128)(2,1)}, bf16[16384,64]{1,0:T(8,128)(2,1)}) fusion(bf16[16384,128]{1,0:T(8,128)(2,1)} %get-tuple-element.194), kind=kLoop, calls=%fused_computation.85 | loop fusion | bytes 8388608 | tf_op jit(solution)/shard_map/split | solution.py:31
  95.9 145.9 %while.17 = (s32[]{:T(128)}, f32[512,1]{0,1:T(1,128)S(1)}, f32[512,1]{0,1:T(1,128)}, f32[512,1,64]{0,2,1:T(8,128)}, s32[512]{0:T(512)S(1)}, /*index=5*/bf16[1638...) while((s32[]{:T(128)}, f32[512,1]{0,1:T(1,128)S(1)}, ...), condition=%wide.region_5.5_spmd.clone, body=%wide.region_2.4_spmd.clone.sunk | while | flops 69833728 | bytes 3784919 | solution.py:90
  96.0 1.3 fusion.82
  98.0 1.9 fusion.85
  99.9 1.3 fusion.82
  102.5 1.9 fusion.85
  104.5 1.3 fusion.82
  107.1 1.9 fusion.85
  109.1 1.3 fusion.82
  111.7 1.9 fusion.85
  116.3 1.9 fusion.85
  118.2 1.3 fusion.82
  120.9 1.9 fusion.85
  122.8 1.3 fusion.82
  125.4 1.9 fusion.85
  127.4 1.3 fusion.82
  130.0 1.9 fusion.85
  134.6 1.9 fusion.85
  136.5 1.3 fusion.82
  139.2 1.9 fusion.85
  141.1 1.3 fusion.82
  143.8 1.9 fusion.85
  148.3 1.9 fusion.85
  152.9 1.9 fusion.85
  157.5 1.9 fusion.85
  162.1 1.9 fusion.85
  166.7 1.9 fusion.85
  171.2 1.9 fusion.85
  175.8 1.9 fusion.85
  180.4 1.9 fusion.85
  185.0 1.9 fusion.85
  189.6 1.9 fusion.85
  194.1 1.9 fusion.85
  198.7 1.9 fusion.85
  203.3 1.9 fusion.85
  207.9 1.9 fusion.85
  212.4 1.9 fusion.85
  217.0 1.9 fusion.85
  221.6 1.9 fusion.85
  226.2 1.9 fusion.85
  230.8 1.9 fusion.85
  235.3 1.9 fusion.85
  239.9 1.9 fusion.85
  243.9 7.1 %all-to-all-start.1 = ((bf16[16,512,64]{1,2,0:T(8,128)(2,1)}), bf16[16,512,64]{1,2,0:T(8,128)(2,1)S(1)}, u32[]{:S(2)}, u32[]{:S(2)}) async-start(bf16[16,512,64]{1,2,0:T(8,128)(2,1)} %broadcast_in_dim.67), calls=%async_computation.1 | async-start | bytes 2097152 | tf_op jit(solution)/shard_map/all_to_all | solution.py:20
  251.5 9.0 %reduce-window.6 = s32[32,8,128]{2,1,0:T(8,128)S(1)} reduce-window(s32[32,8,128]{2,1,0:T(8,128)S(1)} %fusion.61, s32[]{:T(128)} %constant.103.clone.1), window={size=1x1x128 pad=0_0x0_0x127_0}, to_apply=%region_6.7 | reduce-window | flops 4161536 | bytes 262148 | tf_op jit(solution)/shard_map/reduce-window
  261.1 4.3 scatter_custom_fusion
  265.4 2.0 all-to-all-done.1
  267.9 6.2 %gather_fusion = bf16[2048,128]{1,0:T(8,128)(2,1)S(1)} fusion(bf16[513,128]{1,0:T(8,128)(2,1)S(1)} %concatenate.7, s32[2048]{0:T(1024)S(1)} %fusion.63), kind=kCustom, calls=%fused_computation | custom fusion | bytes 1056768 | tf_op jit(solution)/shard_map/gather | solution.py:134
  274.1 42.7 %all_to_all.20 = bf16[32,64,128]{2,1,0:T(8,128)(2,1)} all-to-all(bf16[32,64,128]{2,1,0:T(8,128)(2,1)S(1)} %bitcast.160), channel_id=1, replica_groups=mesh['sp'=32,'tp'=16] {'sp'}, dimensions={0} | all-to-all | bytes 1048576 | tf_op jit(solution)/shard_map/all_to_all | solution.py:135
  317.1 79.2 %all-gather.9.cloned.1.call-done = bf16[32,64,2048]{2,1,0:T(8,128)(2,1)} async-done(((bf16[32,64,128]{2,1,0:T(8,128)(2,1)}), bf16[32,64,2048]{2,1,0:T(8,128)(2,1)}) %all-gather.9.cloned.1.call-update) | async-done | bytes 8388624 | tf_op jit(solution)/shard_map/all_gather | solution.py:138
  396.3 5.2 fusion.19
  402.0 2.7 fusion.32
  404.7 3.7 fusion.47
  408.5 92.1 %all-gather.7.cloned.1.call-done = bf16[32,1,64,2048]{3,2,0,1:T(8,128)(2,1)} async-done(((bf16[32,1,64,128]{3,2,0,1:T(8,128)(2,1)}), bf16[32,1,64,2048]{3,2,0,1:T(8,128)(2,1)}) %all-gather.7.cloned.1.call-update) | async-done | bytes 8388624 | tf_op jit(solution)/shard_map/all_gather | solution.py:153
  500.6 6.6 %fusion.50 = bf16[32,64,128]{2,1,0:T(8,128)(2,1)} fusion(bf16[32,1,64,2048]{3,2,0,1:T(8,128)(2,1)} %all-gather.7.cloned.1.call-done, bf16[1,2048,128]{2,1,0:T(8,128)(2,1)S(1)} %copy-done.9), kind=kOutput, calls=%fused_computation.49 | convolution fusion | flops 1074003968 | bytes 9437184 | tf_op jit(solution)/shard_map/seif,efc->seic/dot_general | solution.py:151
  507.2 14.4 %all-to-all-start.3 = ((bf16[32,64,128]{2,1,0:T(8,128)(2,1)}), bf16[32,64,128]{2,1,0:T(8,128)(2,1)S(1)}, u32[]{:S(2)}, u32[]{:S(2)}) async-start(bf16[32,64,128]{2,1,0:T(8,128)(2,1)} %fusion.50), calls=%async_computation.3 | async-start | bytes 1048576 | tf_op jit(solution)/shard_map/all_to_all | solution.py:157
  521.7 33.3 %all-to-all-done.3 = bf16[32,64,128]{2,1,0:T(8,128)(2,1)S(1)} async-done(((bf16[32,64,128]{2,1,0:T(8,128)(2,1)}), bf16[32,64,128]{2,1,0:T(8,128)(2,1)S(1)}, u32[]{:S(2)}, u32[]{:S(2)}) %all-to-all-start.3) | async-done | bytes 524320 | tf_op jit(solution)/shard_map/all_to_all | solution.py:157
  555.1 3.2 gather_fusion.1
  558.3 2.8 fusion.54
  (277 shorter events, 81.4 us)
Async XLA Ops:
  6.5 395.0 %copy-start = (bf16[1,2048,128]{2,1,0:T(8,128)(2,1)S(1)}, bf16[1,2048,128]{2,1,0:T(8,128)(2,1)}, u32[]{:S(2)}) copy-start(bf16[1,2048,128]{2,1,0:T(8,128)(2,1)} %param.25) | copy-start | bytes 1572868
  6.5 82.0 %all-gather.5.cloned.1.call-start = ((), (), s32[]{:S(2)}) async-start(), calls=%async_computation.4 | async-start | bytes 4325376 | tf_op jit(solution)/shard_map/all_gather | solution.py:30
  10.7 29.8 %all-to-all-start = ((f32[32,512,1]{1,2,0:T(1,128)}), f32[32,512,1]{1,2,0:T(1,128)S(1)}, u32[]{:S(2)}, u32[]{:S(2)}) async-start(f32[32,512,1]{1,2,0:T(1,128)} %broadcast_in_dim.66), calls=%async_computation | async-start | bytes 131072 | tf_op jit(solution)/shard_map/all_to_all | solution.py:20
  88.6 162.4 %copy-start.4 = (s32[512,2]{0,1:T(2,128)S(1)}, s32[512,2]{0,1:T(2,128)}, u32[]{:S(2)}) copy-start(s32[512,2]{0,1:T(2,128)} %param.23) | copy-start | bytes 12292
  88.6 178.8 %copy-start.2 = (bf16[1024,128]{1,0:T(8,128)(2,1)S(1)}, bf16[1024,128]{1,0:T(8,128)(2,1)}, u32[]{:S(2)}) copy-start(bf16[1024,128]{1,0:T(8,128)(2,1)} %param.21) | copy-start | bytes 786436
  88.6 178.8 %copy-start.3 = (bf16[512,128]{1,0:T(8,128)(2,1)S(1)}, bf16[512,128]{1,0:T(8,128)(2,1)}, u32[]{:S(2)}) copy-start(bf16[512,128]{1,0:T(8,128)(2,1)} %param.20) | copy-start | bytes 393220
  88.6 7.3 %copy-start.7 = (f32[512,1]{0,1:T(1,128)S(1)}, f32[512,1]{0,1:T(1,128)}, u32[]{:S(2)}) copy-start(f32[512,1]{0,1:T(1,128)} %get-tuple-element.359) | copy-start | bytes 6148 | tf_op jit(solution)/shard_map/cond
  88.6 7.3 %copy-start.10 = (bf16[512,64]{0,1:T(8,128)(2,1)S(1)}, bf16[512,64]{0,1:T(8,128)(2,1)}, u32[]{:S(2)}) copy-start(bf16[512,64]{0,1:T(8,128)(2,1)} %get-tuple-element.205) | copy-start | bytes 196612 | tf_op jit(solution)/shard_map/cond
  241.8 75.2 %copy-start.6 = (bf16[2048]{0:T(1024)(128)(2,1)S(1)}, bf16[2048]{0:T(1024)(128)(2,1)}, u32[]{:S(2)}) copy-start(bf16[2048]{0:T(1024)(128)(2,1)} %param.22) | copy-start | bytes 12292
  243.9 23.5 %all-to-all-start.1 = ((bf16[16,512,64]{1,2,0:T(8,128)(2,1)}), bf16[16,512,64]{1,2,0:T(8,128)(2,1)S(1)}, u32[]{:S(2)}, u32[]{:S(2)}) async-start(bf16[16,512,64]{1,2,0:T(8,128)(2,1)} %broadcast_in_dim.67), calls=%async_computation.1 | async-start | bytes 2097152 | tf_op jit(solution)/shard_map/all_to_all | solution.py:20
  250.9 145.3 %all-gather.9.cloned.1.call-start = ((), (), s32[]{:S(2)}) async-start(), calls=%async_computation.6 | async-start | bytes 8912896 | tf_op jit(solution)/shard_map/all_gather | solution.py:138
  316.8 183.8 %all-gather.7.cloned.1.call-start = ((), (), s32[]{:S(2)}) async-start(), calls=%async_computation.5 | async-start | bytes 8912896 | tf_op jit(solution)/shard_map/all_gather | solution.py:153
  396.3 5.8 %copy-start.1 = (bf16[32,64,2048]{2,1,0:T(8,128)(2,1)S(1)}, bf16[32,64,2048]{2,1,0:T(8,128)(2,1)}, u32[]{:S(2)}) copy-start(bf16[32,64,2048]{2,1,0:T(8,128)(2,1)} %all-gather.9.cloned.1.call-done) | copy-start | bytes 25165828
  402.0 2.7 copy-start.8
  404.7 95.9 %copy-start.9 = (bf16[1,2048,128]{2,1,0:T(8,128)(2,1)S(1)}, bf16[1,2048,128]{2,1,0:T(8,128)(2,1)}, u32[]{:S(2)}) copy-start(bf16[1,2048,128]{2,1,0:T(8,128)(2,1)} %param.27) | copy-start | bytes 1572868
  408.5 113.1 %copy-start.5 = (f32[512,2]{0,1:T(2,128)S(1)}, f32[512,2]{0,1:T(2,128)}, u32[]{:S(2)}) copy-start(f32[512,2]{0,1:T(2,128)} %param.24) | copy-start | bytes 12292
  507.2 47.9 %all-to-all-start.3 = ((bf16[32,64,128]{2,1,0:T(8,128)(2,1)}), bf16[32,64,128]{2,1,0:T(8,128)(2,1)S(1)}, u32[]{:S(2)}, u32[]{:S(2)}) async-start(bf16[32,64,128]{2,1,0:T(8,128)(2,1)} %fusion.50), calls=%async_computation.3 | async-start | bytes 1048576 | tf_op jit(solution)/shard_map/all_to_all | solution.py:157
Sparse Core Ops, SparseCore 0:
  9.5 79.0 all-gather.4
  316.9 79.2 all-gather.8
  408.6 91.9 all-gather.6
where the time goes:
time: 571 us; the launch traced here: 568 us
  waiting for transfers between devices  267 us (47%)
  matrix products  115 us (20%)
  other arithmetic  63 us (11%)
  blocking collectives  42.7 us (7%)
  starting transfers between devices  38.5 us (7%)
  local copies, waits for them, and re-layouts  28 us (5%)
  between operations  13.4 us (2%)
    all_gather x1, waiting for transfers between devices, body(): lax.all_gather(activated, 'tp', axis=3, tiled=True)  92.1 us
    all_gather x1, waiting for transfers between devices, body(): lax.all_gather(grouped, 'tp', axis=3, tiled=True)  79.2 us
    dot_general x32, matrix products, one_block(): jnp.einsum('qhk,khd->qhd', raised.astype(jnp.bfloat16), value_block, pref...  61.4 us
    all_gather x1, waiting for transfers between devices, side_by_side(): result = lax.all_gather(both, axis, axis=dim, tiled=True)  48.2 us
    all_to_all x1, blocking collectives, body(): lax.all_to_all(outgoing, 'sp', split_axis=0, concat_axis=0, tiled=True)  42.7 us
    dot_general x32, matrix products, one_block(): jnp.einsum('qhd,khd->qhk', queries, key_block, preferred_element_type=jnp...  40.4 us
    add x32, other arithmetic, one_block(): total = total * shrink + jnp.sum(raised, axis=-1)  36.7 us
    all_to_all x1, waiting for transfers between devices, body(): lax.all_to_all(produced.reshape(groups * local_experts, count, down_weigh...  33.3 us
  transfers between devices with their start and end apart: 6, of which 6 were waited for; matrix products, arithmetic and copies ran while one was open for 3% of the time, Pallas kernels for 0%

commit v1 on v0

--- a/solution.py
+++ b/solution.py
@@ -7,6 +7,12 @@
 NORM_EPS = 1e-06
 CLAMP_LIMIT = 7.0
 SILU_ALPHA = 1.702
+
+
+def finish_pairs_all(block_in, peer_axis="tp"):
+    val2 = jnp.stack([block_in for _ in range(lax.axis_size(peer_axis))])
+    right_arr = lax.all_to_all(val2, peer_axis, 0, 0)
+    return jnp.concatenate(right_arr, 3)
 
 
 def joined_along(parts, dim):
@@ -150,7 +156,7 @@
     weight_rows = down_weight
     produced = jnp.einsum(
         "seif,efc->seic",
-        lax.all_gather(activated, "tp", axis=3, tiled=True),
+        finish_pairs_all(activated),
         weight_rows,
         preferred_element_type=jnp.float32,
     ).astype(jnp.bfloat16)

time: 571 us -> 623 us (1.091)
  blocking collectives: 42.7 us -> 143 us
  waiting for transfers between devices: 267 us -> 175 us
  local copies, waits for them, and re-layouts: 28 us -> 66.7 us
    all_to_all x0 -> x1, blocking collectives: none -> 100 us  [finish_pairs_all(): right_arr = lax.all_to_all(val2, peer_axis, 0, 0)]
    all_gather x1 -> x0, waiting for transfers between devices: 92.1 us -> none  [body(): lax.all_gather(activated, 'tp', axis=3, tiled=True)]
    reshape x0 -> x1, local copies, waits for them, and re-layouts: none -> 23.1 us  [finish_pairs_all(): return jnp.concatenate(right_arr, 3)]
    another operation x2 -> x4, local copies, waits for them, and re-layouts: 0.08 us -> 15.6 us
  transfers between devices with their start and end apart: 6 -> 5, of which waited for: 6 -> 5; matrix products, arithmetic and copies ran while one was open for 3% -> 3% of each run, Pallas kernels for 0% -> 0%
where the time goes in v1:
time: 623 us; the launch traced here: 620 us
  waiting for transfers between devices  175 us (28%)
  blocking collectives  143 us (23%)
  matrix products  115 us (18%)
  other arithmetic  67.1 us (11%)
  local copies, waits for them, and re-layouts  66.7 us (11%)
  starting transfers between devices  39.4 us (6%)
  between operations  13.7 us (2%)
    all_to_all x1, blocking collectives, finish_pairs_all(): right_arr = lax.all_to_all(val2, peer_axis, 0, 0)  100 us
    all_gather x1, waiting for transfers between devices, body(): lax.all_gather(grouped, 'tp', axis=3, tiled=True)  79.4 us
    dot_general x32, matrix products, one_block(): jnp.einsum('qhk,khd->qhd', raised.astype(jnp.bfloat16), value_block, pref...  61.5 us
    all_gather x1, waiting for transfers between devices, side_by_side(): result = lax.all_gather(both, axis, axis=dim, tiled=True)  48.2 us
    all_to_all x1, blocking collectives, body(): lax.all_to_all(outgoing, 'sp', split_axis=0, concat_axis=0, tiled=True)  42.7 us
    add x32, other arithmetic, one_block(): total = total * shrink + jnp.sum(raised, axis=-1)  40.8 us
    dot_general x32, matrix products, one_block(): jnp.einsum('qhd,khd->qhk', queries, key_block, preferred_element_type=jnp...  40.8 us
    all_to_all x1, waiting for transfers between devices, body(): lax.all_to_all(produced.reshape(groups * local_experts, count, down_weigh...  33.3 us
  transfers between devices with their start and end apart: 5, of which 5 were waited for; matrix products, arithmetic and copies ran while one was open for 3% of the time, Pallas kernels for 0%

profile of v1, /device:TPU:1, one launch (start us, length us, event | category | flops | bytes accessed | tf_op | source)
XLA Modules:
  0.0 620.0 jit_solution(5338646229577842446)
XLA Ops:
  9.3 1.3 broadcast_in_dim.66
  10.7 16.7 %all-to-all-start = ((f32[32,512,1]{1,2,0:T(1,128)}), f32[32,512,1]{1,2,0:T(1,128)S(1)}, u32[]{:S(2)}, u32[]{:S(2)}) async-start(f32[32,512,1]{1,2,0:T(1,128)} %broadcast_in_dim.66), calls=%async_computation | async-start | bytes 131072 | tf_op jit(solution)/shard_map/all_to_all | solution.py:26
  28.4 12.0 %all-to-all-done = f32[32,512,1]{1,2,0:T(1,128)S(1)} async-done(((f32[32,512,1]{1,2,0:T(1,128)}), f32[32,512,1]{1,2,0:T(1,128)S(1)}, u32[]{:S(2)}, u32[]{:S(2)}) %all-to-all-start) | async-done | bytes 65568 | tf_op jit(solution)/shard_map/all_to_all | solution.py:26
  40.4 48.2 %all-gather.4.cloned.1.call-done = bf16[16384,128]{1,0:T(8,128)(2,1)} async-done(((bf16[512,128]{1,0:T(8,128)(2,1)}), bf16[16384,128]{1,0:T(8,128)(2,1)}) %all-gather.4.cloned.1.call-update) | async-done | bytes 4194320 | tf_op jit(solution)/shard_map/all_gather | solution.py:36
  88.6 157.9 %conditional.1 = (f32[512,1]{0,1:T(1,128)}, f32[512,1,64]{0,2,1:T(8,128)}) conditional(s32[]{:T(128)} %convert_element_type.59, () %tuple.27, (bf16[16384,128]{1,0:T(8,128)(2,1)}, f32[32,512,1]{1,2,0:T(1,128)S(1)}, bf16[512,64]{0,1:T(8,128)(2,1)}, s32[]{:T(128)}, s32[512]{0:T(512)S(1)}, /*index=5*/f32[512,1]{0,1:T(1,128)}) %tuple.28), branch_computations={%region_0.0_spmd, %region_1.6_spmd} | conditional | flops 69834240 | bytes 12448147 | solution.py:101
  88.6 7.3 %fusion.69 = (bf16[16384,64]{1,0:T(8,128)(2,1)}, bf16[16384,64]{1,0:T(8,128)(2,1)}) fusion(bf16[16384,128]{1,0:T(8,128)(2,1)} %get-tuple-element.194), kind=kLoop, calls=%fused_computation.84 | loop fusion | bytes 8388608 | tf_op jit(solution)/shard_map/split | solution.py:37
  96.0 150.5 %while.17 = (s32[]{:T(128)}, f32[512,1]{0,1:T(1,128)S(1)}, f32[512,1]{0,1:T(1,128)}, f32[512,1,64]{0,2,1:T(8,128)}, s32[512]{0:T(512)S(1)}, /*index=5*/bf16[1638...) while((s32[]{:T(128)}, f32[512,1]{0,1:T(1,128)S(1)}, ...), condition=%wide.region_5.5_spmd.clone, body=%wide.region_2.4_spmd.clone.sunk | while | flops 69833728 | bytes 3784911 | solution.py:96
  98.1 1.9 fusion.84
  102.8 1.9 fusion.84
  107.5 1.9 fusion.84
  110.9 1.3 fusion.83
  112.2 1.9 fusion.84
  117.0 1.9 fusion.84
  120.4 1.3 fusion.83
  121.7 1.9 fusion.84
  126.4 1.9 fusion.84
  129.8 1.3 fusion.83
  131.1 1.9 fusion.84
  135.9 1.9 fusion.84
  140.6 1.9 fusion.84
  145.3 1.9 fusion.84
  150.0 1.9 fusion.84
  154.8 1.9 fusion.84
  159.5 1.9 fusion.84
  164.2 1.9 fusion.84
  168.9 1.9 fusion.84
  173.7 1.9 fusion.84
  178.4 1.9 fusion.84
  183.1 1.9 fusion.84
  187.8 1.9 fusion.84
  192.6 1.9 fusion.84
  197.3 1.9 fusion.84
  200.7 1.3 fusion.83
  202.0 1.9 fusion.84
  206.7 1.9 fusion.84
  210.2 1.3 fusion.83
  211.5 1.9 fusion.84
  216.2 1.9 fusion.84
  219.6 1.3 fusion.83
  220.9 1.9 fusion.84
  225.6 1.9 fusion.84
  230.3 1.9 fusion.84
  235.1 1.9 fusion.84
  239.8 1.9 fusion.84
  244.5 1.9 fusion.84
  248.5 7.1 %all-to-all-start.1 = ((bf16[16,512,64]{1,2,0:T(8,128)(2,1)}), bf16[16,512,64]{1,2,0:T(8,128)(2,1)S(1)}, u32[]{:S(2)}, u32[]{:S(2)}) async-start(bf16[16,512,64]{1,2,0:T(8,128)(2,1)} %broadcast_in_dim.67), calls=%async_computation.1 | async-start | bytes 2097152 | tf_op jit(solution)/shard_map/all_to_all | solution.py:26
  255.8 9.0 %reduce-window.6 = s32[32,8,128]{2,1,0:T(8,128)S(1)} reduce-window(s32[32,8,128]{2,1,0:T(8,128)S(1)} %fusion.59, s32[]{:T(128)} %constant.103.clone.1), window={size=1x1x128 pad=0_0x0_0x127_0}, to_apply=%region_6.7 | reduce-window | flops 4161536 | bytes 262148 | tf_op jit(solution)/shard_map/reduce-window
  265.7 4.3 scatter_custom_fusion
  270.0 2.0 all-to-all-done.1
  272.5 6.2 gather_fusion
  278.7 42.7 %all_to_all.25 = bf16[32,64,128]{2,1,0:T(8,128)(2,1)} all-to-all(bf16[32,64,128]{2,1,0:T(8,128)(2,1)S(1)} %bitcast.170), channel_id=1, replica_groups=mesh['sp'=32,'tp'=16] {'sp'}, dimensions={0} | all-to-all | bytes 1048576 | tf_op jit(solution)/shard_map/all_to_all | solution.py:141
  321.4 79.4 %all-gather.6.cloned.1.call-done = bf16[32,64,2048]{2,1,0:T(8,128)(2,1)} async-done(((bf16[32,64,128]{2,1,0:T(8,128)(2,1)}), bf16[32,64,2048]{2,1,0:T(8,128)(2,1)}) %all-gather.6.cloned.1.call-update) | async-done | bytes 8388624 | tf_op jit(solution)/shard_map/all_gather | solution.py:144
  400.8 5.2 fusion.19
  406.6 2.7 fusion.30
  409.3 2.9 fusion.48
  412.2 2.1 stack.2
  414.4 100.0 %all_to_all.26 = bf16[16,32,1,64,128]{4,3,1,2,0:T(8,128)(2,1)} all-to-all(bf16[16,32,1,64,128]{4,3,1,2,0:T(8,128)(2,1)S(1)} %stack.2), channel_id=1, replica_groups=mesh['sp'=32,'tp'=16] {'tp'}, dimensions={0} | all-to-all | bytes 16777216 | tf_op jit(solution)/shard_map/all_to_all | solution.py:14
  514.4 23.1 %copy.36 = bf16[32,1,64,16,128]{4,3,2,0,1:T(8,128)(2,1)} copy(bf16[32,1,64,16,128]{4,2,0,1,3:T(8,128)(2,1)} %bitcast.167) | data formatting | bytes 16777216 | tf_op jit(solution)/shard_map/reshape | solution.py:15
  537.5 13.4 %reshape.237 = bf16[32,64,2048]{2,1,0:T(8,128)(2,1)} reshape(bf16[32,1,64,16,128]{4,3,2,0,1:T(8,128)(2,1)} %copy.36) | data formatting | bytes 16777216 | tf_op jit(solution)/shard_map/reshape.33
  550.9 6.5 %convolution_convert_fusion = bf16[32,64,128]{2,1,0:T(8,128)(2,1)} fusion(bf16[32,64,2048]{2,1,0:T(8,128)(2,1)} %reshape.237, bf16[1,2048,128]{2,1,0:T(8,128)(2,1)S(1)} %copy-done.9), kind=kOutput, calls=%fused_computation.47 | convolution fusion | flops 1074003968 | bytes 9437184 | tf_op jit(solution)/shard_map/seif,efc->seic/dot_general | solution.py:157
  557.4 15.5 %all-to-all-start.4 = ((bf16[32,64,128]{2,1,0:T(8,128)(2,1)}), bf16[32,64,128]{2,1,0:T(8,128)(2,1)S(1)}, u32[]{:S(2)}, u32[]{:S(2)}) async-start(bf16[32,64,128]{2,1,0:T(8,128)(2,1)} %convolution_convert_fusion), calls=%async_computation.4 | async-start | bytes 1048576 | tf_op jit(solution)/shard_map/all_to_all | solution.py:163
  573.1 33.3 %all-to-all-done.4 = bf16[32,64,128]{2,1,0:T(8,128)(2,1)S(1)} async-done(((bf16[32,64,128]{2,1,0:T(8,128)(2,1)}), bf16[32,64,128]{2,1,0:T(8,128)(2,1)S(1)}, u32[]{:S(2)}, u32[]{:S(2)}) %all-to-all-start.4) | async-done | bytes 524320 | tf_op jit(solution)/shard_map/all_to_all | solution.py:163
  606.4 3.2 gather_fusion.1
  609.6 2.8 fusion.52
  (278 shorter events, 89.2 us)
Async XLA Ops:
  6.5 399.5 %copy-start = (bf16[1,2048,128]{2,1,0:T(8,128)(2,1)S(1)}, bf16[1,2048,128]{2,1,0:T(8,128)(2,1)}, u32[]{:S(2)}) copy-start(bf16[1,2048,128]{2,1,0:T(8,128)(2,1)} %param.25) | copy-start | bytes 1572868
  6.5 82.0 %all-gather.4.cloned.1.call-start = ((), (), s32[]{:S(2)}) async-start(), calls=%async_computation.5 | async-start | bytes 4325376 | tf_op jit(solution)/shard_map/all_gather | solution.py:36
  10.7 29.8 %all-to-all-start = ((f32[32,512,1]{1,2,0:T(1,128)}), f32[32,512,1]{1,2,0:T(1,128)S(1)}, u32[]{:S(2)}, u32[]{:S(2)}) async-start(f32[32,512,1]{1,2,0:T(1,128)} %broadcast_in_dim.66), calls=%async_computation | async-start | bytes 131072 | tf_op jit(solution)/shard_map/all_to_all | solution.py:26
  88.6 167.0 %copy-start.4 = (s32[512,2]{0,1:T(2,128)S(1)}, s32[512,2]{0,1:T(2,128)}, u32[]{:S(2)}) copy-start(s32[512,2]{0,1:T(2,128)} %param.23) | copy-start | bytes 12292
  88.6 183.4 %copy-start.2 = (bf16[1024,128]{1,0:T(8,128)(2,1)S(1)}, bf16[1024,128]{1,0:T(8,128)(2,1)}, u32[]{:S(2)}) copy-start(bf16[1024,128]{1,0:T(8,128)(2,1)} %param.21) | copy-start | bytes 786436
  88.6 183.4 %copy-start.3 = (bf16[512,128]{1,0:T(8,128)(2,1)S(1)}, bf16[512,128]{1,0:T(8,128)(2,1)}, u32[]{:S(2)}) copy-start(bf16[512,128]{1,0:T(8,128)(2,1)} %param.20) | copy-start | bytes 393220
  88.6 7.4 %copy-start.7 = (f32[512,1]{0,1:T(1,128)S(1)}, f32[512,1]{0,1:T(1,128)}, u32[]{:S(2)}) copy-start(f32[512,1]{0,1:T(1,128)} %get-tuple-element.359) | copy-start | bytes 6148 | tf_op jit(solution)/shard_map/cond
  88.6 7.4 %copy-start.10 = (bf16[512,64]{0,1:T(8,128)(2,1)S(1)}, bf16[512,64]{0,1:T(8,128)(2,1)}, u32[]{:S(2)}) copy-start(bf16[512,64]{0,1:T(8,128)(2,1)} %get-tuple-element.205) | copy-start | bytes 196612 | tf_op jit(solution)/shard_map/cond
  246.4 75.0 %copy-start.6 = (bf16[2048]{0:T(1024)(128)(2,1)S(1)}, bf16[2048]{0:T(1024)(128)(2,1)}, u32[]{:S(2)}) copy-start(bf16[2048]{0:T(1024)(128)(2,1)} %param.22) | copy-start | bytes 12292
  248.5 23.5 %all-to-all-start.1 = ((bf16[16,512,64]{1,2,0:T(8,128)(2,1)}), bf16[16,512,64]{1,2,0:T(8,128)(2,1)S(1)}, u32[]{:S(2)}, u32[]{:S(2)}) async-start(bf16[16,512,64]{1,2,0:T(8,128)(2,1)} %broadcast_in_dim.67), calls=%async_computation.1 | async-start | bytes 2097152 | tf_op jit(solution)/shard_map/all_to_all | solution.py:26
  255.5 145.3 %all-gather.6.cloned.1.call-start = ((), (), s32[]{:S(2)}) async-start(), calls=%async_computation.6 | async-start | bytes 8912896 | tf_op jit(solution)/shard_map/all_gather | solution.py:144
  400.8 5.8 copy-start.1
  406.6 2.7 copy-start.8
  537.5 13.4 %copy-start.9 = (bf16[1,2048,128]{2,1,0:T(8,128)(2,1)S(1)}, bf16[1,2048,128]{2,1,0:T(8,128)(2,1)}, u32[]{:S(2)}) copy-start(bf16[1,2048,128]{2,1,0:T(8,128)(2,1)} %param.27) | copy-start | bytes 1572868
  550.9 22.0 %copy-start.5 = (f32[512,2]{0,1:T(2,128)S(1)}, f32[512,2]{0,1:T(2,128)}, u32[]{:S(2)}) copy-start(f32[512,2]{0,1:T(2,128)} %param.24) | copy-start | bytes 12292
  557.4 49.0 %all-to-all-start.4 = ((bf16[32,64,128]{2,1,0:T(8,128)(2,1)}), bf16[32,64,128]{2,1,0:T(8,128)(2,1)S(1)}, u32[]{:S(2)}, u32[]{:S(2)}) async-start(bf16[32,64,128]{2,1,0:T(8,128)(2,1)} %convolution_convert_fusion), calls=%async_computation.4 | async-start | bytes 1048576 | tf_op jit(solution)/shard_map/all_to_all | solution.py:163
Sparse Core Ops, SparseCore 0:
  9.5 79.0 all-gather.3
  321.5 79.2 all-gather.5
